TPU v7x, 32 devices: a whole 2x2x4 slice. The times are simulated.
32 devices in a mesh: gr: 2 (over y), sp: 4 (over z), tp: 4 (over x, core).
Axes of the slice: x: 2, y: 2, z: 4, core: 2. Of those that a mesh axis runs over, the one named last changes fastest.
Arguments:
- tokens: bfloat16 [8, 8192, 2048], P(('gr', 'tp'), 'sp'), may hold values from -6 to 6
- kv_weight: bfloat16 [2048, 1024], replicated, may hold values from -0.125 to 0.125
- queries: bfloat16 [8, 1536], P(('gr', 'tp')), may hold values from -6 to 6
- score_offset: float32 [24], replicated, may hold values from -10.5 to -3.5
Outputs:
- cache: bfloat16 [8, 4, 8192, 256], P(('gr', 'tp'), 'sp')
- read: bfloat16 [8, 1536], P(('gr', 'tp'))
All inputs are finite; a program needn't handle non-finite values.
Results may differ from a plain program's by a relative error of at most 0.0085.
Values may be sent and summed in bfloat16 or wider, within the bound.
A program may use at most 64 MiB of HBM per device.

v0:
```python
import jax
import jax.numpy as jnp
from jax import lax
from jax.sharding import PartitionSpec as P

KVH = 8
HD = 64


def prefix(shard, axis, combine, identity):
    size, index = (lax.axis_size(axis), lax.axis_index(axis))
    everything = lax.all_gather(shard, axis)
    start = jnp.broadcast_to(jnp.asarray(identity, shard.dtype), shard.shape)

    def hop(k, before):
        at = size - 1 - k
        reached = at > index
        new = combine(before, everything[at])
        return jnp.where(reached, new, before)

    return lax.fori_loop(0, size, hop, start)


def add_terms(earlier, later):
    return earlier + later


def finish(contribution):
    return lax.psum(contribution, "sp").astype(jnp.bfloat16)


def local(tokens, kv_weight, queries, score_offset):
    seq_count, pos_rows, model_width = tokens.shape
    features = kv_weight.shape[1]
    slot_count = lax.axis_size("sp")
    blocks = slot_count // seq_count
    block_width = features // blocks
    half_blocks = blocks // 2
    heads = score_offset.shape[0]
    group_size = heads // KVH
    per_block = block_width // HD
    projected = jnp.einsum(
        "spd,dcw->scpw",
        tokens,
        kv_weight.reshape(model_width, blocks, block_width),
        preferred_element_type=jnp.float32,
    ).astype(jnp.bfloat16)
    received = lax.all_to_all(
        projected.reshape(slot_count, pos_rows, block_width),
        "sp",
        split_axis=0,
        concat_axis=1,
        tiled=True,
    )
    length = received.shape[1]
    cache = received.reshape(1, 1, length, block_width)
    key_part = projected[:, :half_blocks].reshape(seq_count, half_blocks, pos_rows, per_block, HD)
    value_part = (
        projected[:, half_blocks:]
        .reshape(seq_count, half_blocks, pos_rows, per_block, HD)
        .astype(jnp.float32)
    )
    query_heads = queries.reshape(seq_count, half_blocks, per_block, group_size, HD)
    offsets = score_offset.reshape(half_blocks, per_block, group_size)
    logits = jnp.einsum(
        "scvgd,scpvd->scvgp", query_heads, key_part, preferred_element_type=jnp.float32
    )
    logits = logits * HD ** (-0.5) + offsets[None, :, :, :, None]
    keep_log = jax.nn.log_sigmoid(-logits)
    between = lax.cumsum(keep_log, axis=4, reverse=True) - keep_log
    totals = jnp.sum(keep_log, axis=4)
    later_keep = prefix(totals, "sp", add_terms, jnp.zeros_like(totals))
    weights = jnp.exp(jax.nn.log_sigmoid(logits) + between + later_keep[..., None])
    weighted = jnp.einsum("scvgp,scpvd->scvgd", weights, value_part)
    contribution = weighted.reshape(seq_count, heads * HD)
    return (cache, finish(contribution))


def solution(mesh):
    placed = (P(("gr", "tp"), "sp", None), P(), P(("gr", "tp"), None), P())
    return jax.shard_map(
        local,
        mesh=mesh,
        in_specs=placed,
        out_specs=(P(("gr", "tp"), "sp", None, None), P(("gr", "tp"), None)),
        check_vma=False,
    )
```

profile of v0, /device:TPU:0, one launch (start us, length us, event | category | flops | bytes accessed | tf_op | source)
XLA Modules:
  0.0 152.8 jit_solution(13266032092984651782)
XLA Ops:
  0.6 6.4 %copy.34 = bf16[2048,1024]{0,1:T(8,128)(2,1)} copy(bf16[2048,1024]{1,0:T(8,128)(2,1)} %param.7) | data formatting | bytes 8388608 | tf_op jit(solution)/shard_map/reshape | solution.py:45
  7.1 13.9 %fusion.2 = bf16[4,256,2048]{2,1,0:T(8,128)(2,1)} fusion(bf16[2048,4,256]{0,2,1:T(8,128)(2,1)} %bitcast.41, bf16[1,2048,2048]{2,1,0:T(8,128)(2,1)} %param.6), kind=kOutput, calls=%fused_computation.3 | convolution fusion | flops 8592031744 | bytes 16777216 | tf_op jit(solution)/shard_map/spd,dcw->scpw/dot_general | solution.py:42
  21.0 0.0 copy-start
  21.0 0.0 copy-start.1
  21.0 6.5 %all-to-all-start = ((bf16[4,2048,256]{1,2,0:T(8,128)(2,1)}), bf16[4,2048,256]{1,2,0:T(8,128)(2,1)}, u32[]{:S(2)}, u32[]{:S(2)}) async-start(bf16[4,2048,256]{1,2,0:T(8,128)(2,1)} %bitcast.38), calls=%async_computation | async-start | bytes 8388608 | tf_op jit(solution)/shard_map/all_to_all | solution.py:48
  27.5 0.0 copy-done
  27.5 0.1 reshape.113
  27.6 0.0 copy-done.1
  27.6 0.1 add.81
  27.7 2.8 %fusion.28 = (bf16[1,2,2048,256]{2,3,1,0:T(8,128)(2,1)S(1)}, bf16[1,2,2048,256]{2,3,1,0:T(8,128)(2,1)S(1)}) fusion(bf16[1,4,2048,256]{2,3,1,0:T(8,128)(2,1)} %bitcast.39), kind=kLoop, calls=%fused_computation.29 | loop fusion | bytes 8388608 | tf_op jit(solution)/shard_map/slice | solution.py:57
  30.4 0.7 fusion.24
  31.1 0.1 reshape.123
  31.2 29.8 %reduce-window.6 = f32[1,2,4,3,16,128]{5,4,3,2,1,0:T(8,128)S(1)} reduce-window(f32[1,2,4,3,16,128]{5,4,3,2,1,0:T(8,128)S(1)} %reshape.123, f32[]{:T(128)} %constant.56.clone.1), window={size=1x1x1x1x1x128 pad=0_0x0_0x0_0x0_0x0_0x0_127}, to_apply=%region_0.1 | reduce-window | flops 6242304 | bytes 393220 | tf_op jit(solution)/shard_map/reduce-window
  61.0 0.1 reshape.124
  61.1 0.2 copy.37
  61.3 1.5 reduce-window.9
  62.8 0.1 slice_bitcast_fusion
  62.9 0.1 broadcast.20
  63.0 0.1 reshape.118
  63.1 63.1 %all-gather = f32[8,4,3]{2,1,0:T(4,128)S(1)} all-gather(f32[2,4,3]{2,1,0:T(4,128)S(1)} %neg.35), channel_id=2, replica_groups=mesh['gr'=2,'sp'=4,'tp'=4] {'sp'}, dimensions={0}, use_global_device_ids=true | all-gather | bytes 480 | tf_op jit(solution)/shard_map/all_gather | solution.py:12
  126.2 0.1 copy.32
  126.3 0.2 while.16
  126.5 0.1 copy.33
  126.6 0.9 fusion.11
  127.6 0.1 reshape.120
  127.7 18.9 %psum.7 = bf16[1,1536]{1,0:T(2,128)(2,1)} all-reduce(f32[1,1536]{1,0:T(1,128)S(1)} %reshape.120), channel_id=1, replica_groups=mesh['gr'=2,'sp'=4,'tp'=4] {'sp'}, use_global_device_ids=true, to_apply=%region_5.6 | all-reduce | flops 1536 | bytes 9216 | tf_op jit(solution)/shard_map/psum | solution.py:29
  146.6 0.0 all-to-all-done
  146.6 6.2 %copy.22 = bf16[4,2048,256]{2,1,0:T(8,128)(2,1)} copy(bf16[4,2048,256]{1,2,0:T(8,128)(2,1)} %all-to-all-done) | data formatting | bytes 8388608 | tf_op jit(solution)/shard_map/all_to_all | solution.py:48
  (8 shorter events, 0.1 us)
Async XLA Ops:
  21.0 6.5 %copy-start = (bf16[1,1536]{1,0:T(2,128)(2,1)S(1)}, bf16[1,1536]{1,0:T(2,128)(2,1)}, u32[]{:S(2)}) copy-start(bf16[1,1536]{1,0:T(2,128)(2,1)} %param.8) | copy-start | bytes 9220
  21.0 6.6 %copy-start.1 = (f32[24]{0:T(128)S(1)}, f32[24]{0:T(128)}, u32[]{:S(2)}) copy-start(f32[24]{0:T(128)} %param.9) | copy-start | bytes 292
  21.0 125.6 %all-to-all-start = ((bf16[4,2048,256]{1,2,0:T(8,128)(2,1)}), bf16[4,2048,256]{1,2,0:T(8,128)(2,1)}, u32[]{:S(2)}, u32[]{:S(2)}) async-start(bf16[4,2048,256]{1,2,0:T(8,128)(2,1)} %bitcast.38), calls=%async_computation | async-start | bytes 8388608 | tf_op jit(solution)/shard_map/all_to_all | solution.py:48
where the time goes:
time: 153 us
  blocking collectives  82 us (54%)
  other arithmetic  31.4 us (21%)
  local copies, waits for them, and re-layouts  16.6 us (11%)
  matrix products  15.5 us (10%)
  starting transfers between devices  6.47 us (4%)
    all_gather x1, blocking collectives, prefix(): everything = lax.all_gather(shard, axis)  63.1 us
    another operation x2, other arithmetic  31.3 us
    psum x1, blocking collectives, finish(): return lax.psum(contribution, 'sp').astype(jnp.bfloat16)  18.9 us
    dot_general x1, matrix products, local(): jnp.einsum('spd,dcw->scpw', tokens, kv_weight.reshape(model_width, blocks...  13.9 us
    all_to_all x1, starting transfers between devices, local(): lax.all_to_all(projected.reshape(slot_count, pos_rows, block_width), 'sp'...  6.47 us
    reshape x1, local copies, waits for them, and re-layouts, local(): kv_weight.reshape(model_width, blocks, block_width)  6.43 us
    all_to_all x1, local copies, waits for them, and re-layouts, local(): lax.all_to_all(projected.reshape(slot_count, pos_rows, block_width), 'sp'...  6.18 us
  transfers between devices with their start and end apart: 1, of which 0 were waited for; matrix products, arithmetic and copies ran while one was open for 24% of the time, Pallas kernels for 0%

commit v1 on v0

--- a/solution.py
+++ b/solution.py
@@ -1,6 +1,10 @@
+import functools
+
 import jax
 import jax.numpy as jnp
 from jax import lax
+from jax.experimental import pallas as pl
+from jax.experimental.pallas import tpu as pltpu
 from jax.sharding import PartitionSpec as P
 
 KVH = 8
@@ -29,7 +33,7 @@
     return lax.psum(contribution, "sp").astype(jnp.bfloat16)
 
 
-def local(tokens, kv_weight, queries, score_offset):
+def local_plain(tokens, kv_weight, queries, score_offset):
     seq_count, pos_rows, model_width = tokens.shape
     features = kv_weight.shape[1]
     slot_count = lax.axis_size("sp")
@@ -76,6 +80,317 @@
     return (cache, finish(contribution))
 
 
+CHUNK = 256
+LANES = 128
+MESH = pl.DeviceIdType.MESH
+
+
+def exchange_kernel(
+    count,
+    tok_hbm,
+    w_hbm,
+    q_ref,
+    off_ref,
+    recv,
+    read_ref,
+    tok,
+    wts,
+    proj,
+    qbig,
+    part,
+    parts,
+    tok_sem,
+    w_sem,
+    send_sem,
+    recv_sem,
+    psend_sem,
+    precv_sem,
+):
+    me = lax.axis_index("sp")
+    rows = tok.shape[0]
+    width = wts.shape[2]
+    chunks = rows // CHUNK
+    heads = q_ref.shape[0]
+    group = heads // KVH
+    half = count // 2
+
+    def dest(j):
+        return lax.rem(me + 1 + j, count)
+
+    def tok_copy(c):
+        at = pl.ds(pl.multiple_of(c * CHUNK, CHUNK), CHUNK)
+        return pltpu.make_async_copy(tok_hbm.at[at, :], tok.at[at, :], tok_sem.at[c])
+
+    def w_copy(d):
+        at = pl.ds(pl.multiple_of(d * width, width), width)
+        return pltpu.make_async_copy(w_hbm.at[:, at], wts.at[d], w_sem.at[d])
+
+    tok_copy(chunks - 1).start()
+    for j in range(count):
+        w_copy(dest(j)).start()
+
+    @pl.loop(1, chunks)
+    def _(i):
+        tok_copy(chunks - 1 - i).start()
+
+    barrier = pltpu.get_barrier_semaphore()
+    for j in range(count - 1):
+        pl.semaphore_signal(barrier, inc=1, device_id={"sp": dest(j)}, device_id_type=MESH)
+
+    spread = jnp.concatenate([q_ref[...].astype(jnp.float32)] * KVH, axis=1)
+    column = lax.broadcasted_iota(jnp.int32, spread.shape, 1) // HD
+    row = lax.broadcasted_iota(jnp.int32, spread.shape, 0) // group
+    mine = column == row
+    qbig[...] = jnp.where(mine, spread, 0.0).astype(jnp.bfloat16)
+    earlier = lax.broadcasted_iota(jnp.int32, (CHUNK, CHUNK), 1)
+    later = lax.broadcasted_iota(jnp.int32, (CHUNK, CHUNK), 0)
+    after = jnp.where(later > earlier, 1.0, 0.0).astype(jnp.bfloat16)
+
+    pl.semaphore_wait(barrier, count - 1)
+
+    interior = jnp.logical_and(me > 0, me < count - 1)
+
+    def adjacent(d):
+        return jnp.logical_or(d == me + 1, d == me - 1)
+
+    def block_copy(d, c):
+        here = pl.ds(pl.multiple_of(c * CHUNK, CHUNK), CHUNK)
+        there = pl.ds(pl.multiple_of(me * rows + c * CHUNK, CHUNK), CHUNK)
+        return pltpu.make_async_remote_copy(
+            src_ref=proj.at[d, here, :],
+            dst_ref=recv.at[there, :],
+            send_sem=send_sem.at[d],
+            recv_sem=recv_sem.at[me],
+            device_id={"sp": d},
+            device_id_type=MESH,
+        )
+
+    def step(i, state):
+        kept, total = state
+        c = chunks - 1 - i
+        at = pl.ds(pl.multiple_of(c * CHUNK, CHUNK), CHUNK)
+        tok_copy(c).wait()
+        for j in range(count):
+            d = dest(j)
+
+            @pl.when(i == 0)
+            def _():
+                w_copy(d).wait()
+
+            block = jnp.dot(
+                tok[at, :], wts[d], preferred_element_type=jnp.float32
+            ).astype(jnp.bfloat16)
+            proj[d, at, :] = block
+            if j == count - 1:
+                own = pl.ds(pl.multiple_of(me * rows + c * CHUNK, CHUNK), CHUNK)
+                recv[own, :] = block
+            if j > 0:
+                before = dest(j - 1)
+
+                @pl.when(jnp.logical_or(interior, adjacent(before)))
+                def _():
+                    block_copy(before, c).start()
+
+        logits = jnp.zeros((heads, CHUNK), jnp.float32)
+        for b in range(half):
+            logits = logits + lax.dot_general(
+                qbig[:, b * width : (b + 1) * width],
+                proj[b, at, :],
+                (((1,), (1,)), ((), ())),
+                preferred_element_type=jnp.float32,
+            )
+        logits = logits * HD ** (-0.5) + off_ref[...]
+        keep = -(jnp.maximum(logits, 0.0) + jnp.log1p(jnp.exp(-jnp.abs(logits))))
+        high = keep.astype(jnp.bfloat16)
+        rest = keep - high.astype(jnp.float32)
+        mid = rest.astype(jnp.bfloat16)
+        low = (rest - mid.astype(jnp.float32)).astype(jnp.bfloat16)
+        sums = jnp.dot(
+            jnp.concatenate([high, mid, low], axis=0), after, preferred_element_type=jnp.float32
+        )
+        between = sums[:heads] + sums[heads : 2 * heads] + sums[2 * heads :]
+        weight = jnp.exp(logits + keep + between + kept)
+        weight_high = weight.astype(jnp.bfloat16)
+        weight_low = (weight - weight_high.astype(jnp.float32)).astype(jnp.bfloat16)
+        both = jnp.concatenate([weight_high, weight_low], axis=0)
+        summed = jnp.concatenate(
+            [
+                jnp.dot(both, proj[half + b, at, :], preferred_element_type=jnp.float32)
+                for b in range(half)
+            ],
+            axis=1,
+        )
+        total = total + summed[:heads] + summed[heads:]
+        kept = kept + jnp.sum(keep, axis=1, keepdims=True)
+        return kept, total
+
+    kept, total = lax.fori_loop(
+        0,
+        chunks,
+        step,
+        (jnp.zeros((heads, 1), jnp.float32), jnp.zeros((heads, KVH * HD), jnp.float32)),
+    )
+    total = jnp.where(mine, total, 0.0)
+    folded = total[:, :LANES]
+    for g in range(1, KVH * HD // LANES):
+        folded = folded + total[:, g * LANES : (g + 1) * LANES]
+    spread_kept = jnp.broadcast_to(kept, (heads, LANES))
+    part[0] = folded
+    part[1] = spread_kept
+    parts[me, 0] = folded
+    parts[me, 1] = spread_kept
+
+    @pl.when(jnp.logical_not(interior))
+    def _():
+        @pl.loop(0, 1)
+        def _(i):
+            for j in range(count - 1):
+                d = dest(j)
+
+                @pl.when(jnp.logical_not(adjacent(d)))
+                def _():
+                    block_copy(d, chunks - 1 - i).start()
+
+    def part_copy(d):
+        return pltpu.make_async_remote_copy(
+            src_ref=part,
+            dst_ref=parts.at[me],
+            send_sem=psend_sem.at[d],
+            recv_sem=precv_sem.at[me],
+            device_id={"sp": d},
+            device_id_type=MESH,
+        )
+
+    for j in range(count - 1):
+        part_copy(dest(j)).start()
+
+    @pl.when(jnp.logical_not(interior))
+    def _():
+        @pl.loop(1, chunks)
+        def _(i):
+            for j in range(count - 1):
+                d = dest(j)
+
+                @pl.when(jnp.logical_not(adjacent(d)))
+                def _():
+                    block_copy(d, chunks - 1 - i).start()
+
+    for j in range(count - 1):
+        d = dest(j)
+        pltpu.make_async_remote_copy(
+            src_ref=part,
+            dst_ref=parts.at[d],
+            send_sem=psend_sem.at[d],
+            recv_sem=precv_sem.at[d],
+            device_id={"sp": d},
+            device_id_type=MESH,
+        ).wait()
+    left = jnp.zeros((heads, LANES), jnp.float32)
+    out = jnp.zeros((heads, LANES), jnp.float32)
+    for z in range(count - 1, -1, -1):
+        out = out + jnp.exp(left) * parts[z, 0]
+        left = left + parts[z, 1]
+    turned = pltpu.roll(out, HD, axis=1)
+    low_half = lax.broadcasted_iota(jnp.int32, (1, LANES), 1) < HD
+    for m in range(heads // 2):
+        first, second = 2 * m, 2 * m + 1
+        from_first = out if (first // group) % 2 == 0 else turned
+        from_second = out if (second // group) % 2 == 1 else turned
+        piece = jnp.where(
+            low_half, from_first[first : first + 1], from_second[second : second + 1]
+        )
+        read_ref[:, m * LANES : (m + 1) * LANES] = piece.astype(read_ref.dtype)
+    for j in range(count - 1):
+        d = dest(j)
+        pltpu.make_async_remote_copy(
+            src_ref=proj.at[d],
+            dst_ref=recv.at[pl.ds(pl.multiple_of(d * rows, CHUNK), rows), :],
+            send_sem=send_sem.at[d],
+            recv_sem=recv_sem.at[d],
+            device_id={"sp": d},
+            device_id_type=MESH,
+        ).wait()
+
+
+def place_kernel(count, got, read, cache, read_out, sems):
+    rows = got.shape[0] // count
+    copies = []
+    for k in range(count):
+        at = pl.ds(k * rows, rows)
+        copies.append(pltpu.make_async_copy(got.at[at, :], cache.at[at, :], sems.at[k]))
+    copies.append(pltpu.make_async_copy(read, read_out, sems.at[count]))
+    for copy in copies:
+        copy.start()
+    for copy in copies:
+        copy.wait()
+
+
+def local(tokens, kv_weight, queries, score_offset):
+    seq_count, rows, model_width = tokens.shape
+    features = kv_weight.shape[1]
+    heads = score_offset.shape[0]
+    count = lax.axis_size("sp")
+    width = features // (count // seq_count)
+    fits = (
+        seq_count == 1
+        and count % 2 == 0
+        and count > 2
+        and width % LANES == 0
+        and rows % CHUNK == 0
+        and features == 2 * KVH * HD
+        and 2 * HD == LANES
+        and heads % 2 == 0
+    )
+    if not fits:
+        return local_plain(tokens, kv_weight, queries, score_offset)
+    length = rows * count
+    vmem = pl.BlockSpec(memory_space=pltpu.VMEM)
+    hbm = pl.BlockSpec(memory_space=pltpu.HBM)
+    got, read = pl.pallas_call(
+        functools.partial(exchange_kernel, count),
+        out_shape=(
+            pltpu.VMEM((length, width), jnp.bfloat16),
+            pltpu.VMEM((1, heads * HD), jnp.bfloat16),
+        ),
+        in_specs=[hbm, hbm, vmem, vmem],
+        out_specs=(vmem, vmem),
+        scratch_shapes=[
+            pltpu.VMEM((rows, model_width), jnp.bfloat16),
+            pltpu.VMEM((count, model_width, width), jnp.bfloat16),
+            pltpu.VMEM((count, rows, width), jnp.bfloat16),
+            pltpu.VMEM((heads, KVH * HD), jnp.bfloat16),
+            pltpu.VMEM((2, heads, LANES), jnp.float32),
+            pltpu.VMEM((count, 2, heads, LANES), jnp.float32),
+            pltpu.SemaphoreType.DMA((rows // CHUNK,)),
+            pltpu.SemaphoreType.DMA((count,)),
+            pltpu.SemaphoreType.DMA((count,)),
+            pltpu.SemaphoreType.DMA((count,)),
+            pltpu.SemaphoreType.DMA((count,)),
+            pltpu.SemaphoreType.DMA((count,)),
+        ],
+        compiler_params=pltpu.CompilerParams(
+            collective_id=0, has_side_effects=True, vmem_limit_bytes=44 * 2**20
+        ),
+    )(
+        tokens.reshape(rows, model_width),
+        kv_weight,
+        queries.reshape(heads, HD),
+        score_offset.reshape(heads, 1),
+    )
+    cache, read = pl.pallas_call(
+        functools.partial(place_kernel, count),
+        out_shape=(
+            jax.ShapeDtypeStruct((length, width), jnp.bfloat16),
+            jax.ShapeDtypeStruct((1, heads * HD), jnp.bfloat16),
+        ),
+        in_specs=[vmem, vmem],
+        out_specs=(hbm, hbm),
+        scratch_shapes=[pltpu.SemaphoreType.DMA((count + 1,))],
+        compiler_params=pltpu.CompilerParams(vmem_limit_bytes=8 * 2**20),
+    )(got, read)
+    return cache.reshape(1, 1, length, width), read
+
+
 def solution(mesh):
     placed = (P(("gr", "tp"), "sp", None), P(), P(("gr", "tp"), None), P())
     return jax.shard_map(

time: 153 us -> 108 us (0.71)
  Pallas kernels: 0 us -> 103 us
  blocking collectives: 82 us -> 0 us
  other arithmetic: 31.4 us -> 0.72 us
  matrix products: 15.5 us -> 0 us
  local copies, waits for them, and re-layouts: 16.6 us -> 3.01 us
  starting transfers between devices: 6.47 us -> 0 us
    pallas_call x0 -> x2, Pallas kernels: none -> 103 us  [the longest x1 101 us: local(): pl.pallas_call(functools.partial(exchange_kernel, count), out_shape=(pltp...]
    all_gather x1 -> x0, blocking collectives: 63.1 us -> none  [prefix(): everything = lax.all_gather(shard, axis)]
    another operation x2 -> x0, other arithmetic: 31.3 us -> none
    psum x1 -> x0, blocking collectives: 18.9 us -> none  [finish(): return lax.psum(contribution, 'sp').astype(jnp.bfloat16)]
    dot_general x3 -> x0, matrix products: 15.5 us -> none  [the longest x1 13.9 us: local(): jnp.einsum('spd,dcw->scpw', tokens, kv_weight.reshape(model_width, blocks...]
    all_to_all x1 -> x0, starting transfers between devices: 6.47 us -> none  [local(): lax.all_to_all(projected.reshape(slot_count, pos_rows, block_width), 'sp'...]
    all_to_all x1 -> x0, local copies, waits for them, and re-layouts: 6.18 us -> none  [local(): lax.all_to_all(projected.reshape(slot_count, pos_rows, block_width), 'sp'...]
    reshape x3 -> x2, local copies, waits for them, and re-layouts: 6.66 us -> 0.82 us  [the longest x1 0.73 us: local(): score_offset.reshape(heads, 1)]
  transfers between devices with their start and end apart: 1 -> 0, of which waited for: 0 -> 0; matrix products, arithmetic and copies ran while one was open for 24% -> 0% of each run, Pallas kernels for 0% -> 0%
where the time goes in v1:
time: 108 us; the launch traced here: 107 us
  Pallas kernels  103 us (95%)
  local copies, waits for them, and re-layouts  3.01 us (3%)
    pallas_call x1, Pallas kernels, local(): pl.pallas_call(functools.partial(exchange_kernel, count), out_shape=(pltp...  101 us
    unnamed x2, local copies, waits for them, and re-layouts  2.19 us

profile of v1, /device:TPU:0, one launch (start us, length us, event | category | flops | bytes accessed | tf_op | source)
XLA Modules:
  0.0 107.3 jit_solution(13904850885518516165)
XLA Ops:
  0.6 0.7 reduce
  1.4 0.1 reshape.17.q_ref
  1.4 0.7 copy.6.off_ref
  2.2 0.0 copy-start
  2.2 2.2 %copy-done = bf16[2048,1024]{1,0:T(8,128)(2,1)S(1)} copy-done((bf16[2048,1024]{1,0:T(8,128)(2,1)S(1)}, bf16[2048,1024]{1,0:T(8,128)(2,1)}, u32[]{:S(2)}) %copy-start) | copy-done | bytes 4194328
  4.4 100.9 %shard_map.59 = (bf16[8192,256]{1,0:T(8,128)(2,1)S(1)}, bf16[1,1536]{1,0:T(2,128)(2,1)S(1)}) custom-call(bf16[2048,2048]{1,0:T(8,128)(2,1)} %bitcast.3, bf16[2048,1024]{1,0:T(8,128)(2,1)S(1)} %copy-done, bf16[24,64]{1,0:T(8,128)(2,1)S(1)} %reshape.17.q_ref, f32[24,1]{1,0:T(8,128)S(1)} %copy.6.off_ref), custom_call_target="tpu_custom_call" | custom-call | tf_op jit(solution)/shard_map/pallas_call | solution.py:349
  105.3 2.1 %shard_map.60 = (bf16[8192,256]{1,0:T(8,128)(2,1)}, bf16[1,1536]{1,0:T(2,128)(2,1)}) custom-call(bf16[8192,256]{1,0:T(8,128)(2,1)S(1)} %get-tuple-element.6.got, bf16[1,1536]{1,0:T(2,128)(2,1)S(1)} %get-tuple-element.7.read), custom_call_target="tpu_custom_call" | custom-call | tf_op jit(solution)/shard_map/pallas_call | solution.py:380
Async XLA Ops:
  2.2 2.2 %copy-start = (bf16[2048,1024]{1,0:T(8,128)(2,1)S(1)}, bf16[2048,1024]{1,0:T(8,128)(2,1)}, u32[]{:S(2)}) copy-start(bf16[2048,1024]{1,0:T(8,128)(2,1)} %w_hbm.1) | copy-start | bytes 12582916

commit v2 on v1

--- a/solution.py
+++ b/solution.py
@@ -81,6 +81,7 @@
 
 
 CHUNK = 256
+VMEM_LIMIT = 56 * 2**20
 LANES = 128
 MESH = pl.DeviceIdType.MESH
 
@@ -110,12 +111,14 @@
     rows = tok.shape[0]
     width = wts.shape[2]
     chunks = rows // CHUNK
-    heads = q_ref.shape[0]
+    heads = off_ref.shape[1]
     group = heads // KVH
     half = count // 2
 
+    way = jnp.where(me < count // 2, 1, -1)
+
     def dest(j):
-        return lax.rem(me + 1 + j, count)
+        return lax.rem(me + count + way * (1 + j), count)
 
     def tok_copy(c):
         at = pl.ds(pl.multiple_of(c * CHUNK, CHUNK), CHUNK)
@@ -137,7 +140,20 @@
     for j in range(count - 1):
         pl.semaphore_signal(barrier, inc=1, device_id={"sp": dest(j)}, device_id_type=MESH)
 
-    spread = jnp.concatenate([q_ref[...].astype(jnp.float32)] * KVH, axis=1)
+    q_rows = []
+    for h in range(heads):
+        pair = q_ref[:, h // 2 * LANES : (h // 2 + 1) * LANES].astype(jnp.float32)
+        q_rows.append(pair if h % 2 == h // group % 2 else pltpu.roll(pair, HD, axis=1))
+    spread = jnp.concatenate(
+        [jnp.concatenate(q_rows, axis=0)] * (KVH * HD // LANES), axis=1
+    )
+    square = (heads, heads)
+    diagonal = lax.broadcasted_iota(jnp.int32, square, 0) == lax.broadcasted_iota(
+        jnp.int32, square, 1
+    )
+    offsets = jnp.sum(
+        jnp.where(diagonal, jnp.broadcast_to(off_ref[...], square), 0.0), axis=1, keepdims=True
+    )
     column = lax.broadcasted_iota(jnp.int32, spread.shape, 1) // HD
     row = lax.broadcasted_iota(jnp.int32, spread.shape, 0) // group
     mine = column == row
@@ -145,8 +161,6 @@
     earlier = lax.broadcasted_iota(jnp.int32, (CHUNK, CHUNK), 1)
     later = lax.broadcasted_iota(jnp.int32, (CHUNK, CHUNK), 0)
     after = jnp.where(later > earlier, 1.0, 0.0).astype(jnp.bfloat16)
-
-    pl.semaphore_wait(barrier, count - 1)
 
     interior = jnp.logical_and(me > 0, me < count - 1)
 
@@ -186,6 +200,11 @@
                 recv[own, :] = block
             if j > 0:
                 before = dest(j - 1)
+                if j == 1:
+
+                    @pl.when(i == 0)
+                    def _():
+                        pl.semaphore_wait(barrier, count - 1)
 
                 @pl.when(jnp.logical_or(interior, adjacent(before)))
                 def _():
@@ -199,7 +218,7 @@
                 (((1,), (1,)), ((), ())),
                 preferred_element_type=jnp.float32,
             )
-        logits = logits * HD ** (-0.5) + off_ref[...]
+        logits = logits * HD ** (-0.5) + offsets
         keep = -(jnp.maximum(logits, 0.0) + jnp.log1p(jnp.exp(-jnp.abs(logits))))
         high = keep.astype(jnp.bfloat16)
         rest = keep - high.astype(jnp.float32)
@@ -369,13 +388,13 @@
             pltpu.SemaphoreType.DMA((count,)),
         ],
         compiler_params=pltpu.CompilerParams(
-            collective_id=0, has_side_effects=True, vmem_limit_bytes=44 * 2**20
+            collective_id=0, has_side_effects=True, vmem_limit_bytes=VMEM_LIMIT
         ),
     )(
         tokens.reshape(rows, model_width),
         kv_weight,
-        queries.reshape(heads, HD),
-        score_offset.reshape(heads, 1),
+        queries,
+        score_offset.reshape(1, heads),
     )
     cache, read = pl.pallas_call(
         functools.partial(place_kernel, count),

time: 108 us -> 104 us (0.963)
  local copies, waits for them, and re-layouts: 3.01 us -> 0 us
    unnamed x2 -> x0, local copies, waits for them, and re-layouts: 2.19 us -> none
where the time goes in v2:
time: 104 us
  Pallas kernels  103 us (99%)
    pallas_call x1, Pallas kernels, local(): pl.pallas_call(functools.partial(exchange_kernel, count), out_shape=(pltp...  101 us

profile of v2, /device:TPU:0, one launch (start us, length us, event | category | flops | bytes accessed | tf_op | source)
XLA Modules:
  0.0 103.7 jit_solution(11376783644236276663)
XLA Ops:
  0.6 101.0 %shard_map.59 = (bf16[8192,256]{1,0:T(8,128)(2,1)S(1)}, bf16[1,1536]{1,0:T(2,128)(2,1)S(1)}) custom-call(bf16[2048,2048]{1,0:T(8,128)(2,1)} %bitcast.3, bf16[2048,1024]{1,0:T(8,128)(2,1)} %w_hbm.1, bf16[1,1536]{1,0:T(2,128)(2,1)} %q_ref.1, f32[1,24]{1,0:T(1,128)} %bitcast.4), custom_call_target="tpu_custom_call" | custom-call | tf_op jit(solution)/shard_map/pallas_call | solution.py:368
  101.6 2.1 %shard_map.60 = (bf16[8192,256]{1,0:T(8,128)(2,1)}, bf16[1,1536]{1,0:T(2,128)(2,1)}) custom-call(bf16[8192,256]{1,0:T(8,128)(2,1)S(1)} %get-tuple-element.6.got, bf16[1,1536]{1,0:T(2,128)(2,1)S(1)} %get-tuple-element.7.read), custom_call_target="tpu_custom_call" | custom-call | tf_op jit(solution)/shard_map/pallas_call | solution.py:399

commit v3 on v2

--- a/solution.py
+++ b/solution.py
@@ -80,7 +80,7 @@
     return (cache, finish(contribution))
 
 
-CHUNK = 256
+CHUNK = 128
 VMEM_LIMIT = 56 * 2**20
 LANES = 128
 MESH = pl.DeviceIdType.MESH
@@ -129,12 +129,8 @@
         return pltpu.make_async_copy(w_hbm.at[:, at], wts.at[d], w_sem.at[d])
 
     tok_copy(chunks - 1).start()
-    for j in range(count):
+    for j in range(2):
         w_copy(dest(j)).start()
-
-    @pl.loop(1, chunks)
-    def _(i):
-        tok_copy(chunks - 1 - i).start()
 
     barrier = pltpu.get_barrier_semaphore()
     for j in range(count - 1):
@@ -162,10 +158,9 @@
     later = lax.broadcasted_iota(jnp.int32, (CHUNK, CHUNK), 0)
     after = jnp.where(later > earlier, 1.0, 0.0).astype(jnp.bfloat16)
 
-    interior = jnp.logical_and(me > 0, me < count - 1)
-
-    def adjacent(d):
-        return jnp.logical_or(d == me + 1, d == me - 1)
+    def deferred(d):
+        inner = jnp.logical_and(d > 0, d < count - 1)
+        return jnp.logical_and(inner, (d < count // 2) != (me < count // 2))
 
     def block_copy(d, c):
         here = pl.ds(pl.multiple_of(c * CHUNK, CHUNK), CHUNK)
@@ -190,6 +185,16 @@
             @pl.when(i == 0)
             def _():
                 w_copy(d).wait()
+                if j == 0:
+                    for k in range(2, count):
+                        w_copy(dest(k)).start()
+                    tok_copy(c - 1).start()
+
+            if j == 0:
+
+                @pl.when(i + 2 < chunks)
+                def _():
+                    tok_copy(c - 2).start()
 
             block = jnp.dot(
                 tok[at, :], wts[d], preferred_element_type=jnp.float32
@@ -206,7 +211,7 @@
                     def _():
                         pl.semaphore_wait(barrier, count - 1)
 
-                @pl.when(jnp.logical_or(interior, adjacent(before)))
+                @pl.when(jnp.logical_not(deferred(before)))
                 def _():
                     block_copy(before, c).start()
 
@@ -259,16 +264,14 @@
     parts[me, 0] = folded
     parts[me, 1] = spread_kept
 
-    @pl.when(jnp.logical_not(interior))
-    def _():
-        @pl.loop(0, 1)
-        def _(i):
-            for j in range(count - 1):
-                d = dest(j)
-
-                @pl.when(jnp.logical_not(adjacent(d)))
-                def _():
-                    block_copy(d, chunks - 1 - i).start()
+    @pl.loop(0, 1)
+    def _(i):
+        for j in range(count - 1):
+            d = dest(j)
+
+            @pl.when(deferred(d))
+            def _():
+                block_copy(d, chunks - 1 - i).start()
 
     def part_copy(d):
         return pltpu.make_async_remote_copy(
@@ -283,16 +286,14 @@
     for j in range(count - 1):
         part_copy(dest(j)).start()
 
-    @pl.when(jnp.logical_not(interior))
-    def _():
-        @pl.loop(1, chunks)
-        def _(i):
-            for j in range(count - 1):
-                d = dest(j)
-
-                @pl.when(jnp.logical_not(adjacent(d)))
-                def _():
-                    block_copy(d, chunks - 1 - i).start()
+    @pl.loop(1, chunks)
+    def _(i):
+        for j in range(count - 1):
+            d = dest(j)
+
+            @pl.when(deferred(d))
+            def _():
+                block_copy(d, chunks - 1 - i).start()
 
     for j in range(count - 1):
         d = dest(j)
@@ -356,6 +357,7 @@
         and count > 2
         and width % LANES == 0
         and rows % CHUNK == 0
+        and rows >= 2 * CHUNK
         and features == 2 * KVH * HD
         and 2 * HD == LANES
         and heads % 2 == 0

time: 104 us -> 102 us (0.981)
  the two profiles are of different devices: /device:TPU:0 before, /device:TPU:9 now
where the time goes in v3:
time: 102 us
  Pallas kernels  101 us (99%)
    pallas_call x1, Pallas kernels, local(): pl.pallas_call(functools.partial(exchange_kernel, count), out_shape=(pltp...  98.8 us
    pallas_call x1, Pallas kernels, local(): pl.pallas_call(functools.partial(place_kernel, count), out_shape=(jax.Sha...  2.05 us

profile of v3, /device:TPU:9, one launch (start us, length us, event | category | flops | bytes accessed | tf_op | source)
XLA Modules:
  0.0 101.5 jit_solution(5419091074048805412)
XLA Ops:
  0.6 98.8 %shard_map.59 = (bf16[8192,256]{1,0:T(8,128)(2,1)S(1)}, bf16[1,1536]{1,0:T(2,128)(2,1)S(1)}) custom-call(bf16[2048,2048]{1,0:T(8,128)(2,1)} %bitcast.3, bf16[2048,1024]{1,0:T(8,128)(2,1)} %w_hbm.1, bf16[1,1536]{1,0:T(2,128)(2,1)} %q_ref.1, f32[1,24]{1,0:T(1,128)} %bitcast.4), custom_call_target="tpu_custom_call" | custom-call | tf_op jit(solution)/shard_map/pallas_call | solution.py:370
  99.5 2.1 %shard_map.60 = (bf16[8192,256]{1,0:T(8,128)(2,1)}, bf16[1,1536]{1,0:T(2,128)(2,1)}) custom-call(bf16[8192,256]{1,0:T(8,128)(2,1)S(1)} %get-tuple-element.6.got, bf16[1,1536]{1,0:T(2,128)(2,1)S(1)} %get-tuple-element.7.read), custom_call_target="tpu_custom_call" | custom-call | tf_op jit(solution)/shard_map/pallas_call | solution.py:401

commit v4 on v3

--- a/solution.py
+++ b/solution.py
@@ -115,10 +115,17 @@
     group = heads // KVH
     half = count // 2
 
-    way = jnp.where(me < count // 2, 1, -1)
+    lower = me < count // 2
 
     def dest(j):
-        return lax.rem(me + count + way * (1 + j), count)
+        if j == count - 1:
+            return me
+        down = count - 1 - j
+        return jnp.where(
+            lower,
+            jnp.where(down > me, down, down - 1),
+            jnp.where(j < me, j, j + 1),
+        )
 
     def tok_copy(c):
         at = pl.ds(pl.multiple_of(c * CHUNK, CHUNK), CHUNK)
@@ -128,13 +135,13 @@
         at = pl.ds(pl.multiple_of(d * width, width), width)
         return pltpu.make_async_copy(w_hbm.at[:, at], wts.at[d], w_sem.at[d])
 
+    barrier = pltpu.get_barrier_semaphore()
+    for j in range(count - 1):
+        pl.semaphore_signal(barrier, inc=1, device_id={"sp": dest(j)}, device_id_type=MESH)
+
     tok_copy(chunks - 1).start()
     for j in range(2):
         w_copy(dest(j)).start()
-
-    barrier = pltpu.get_barrier_semaphore()
-    for j in range(count - 1):
-        pl.semaphore_signal(barrier, inc=1, device_id={"sp": dest(j)}, device_id_type=MESH)
 
     q_rows = []
     for h in range(heads):

time: 102 us -> 101 us (level)
  the two profiles are of different devices: /device:TPU:9 before, /device:TPU:8 now
where the time goes in v4:
time: 101 us; the launch traced here: 100 us
  Pallas kernels  99.7 us (99%)
    pallas_call x1, Pallas kernels, local(): pl.pallas_call(functools.partial(exchange_kernel, count), out_shape=(pltp...  97.7 us
    pallas_call x1, Pallas kernels, local(): pl.pallas_call(functools.partial(place_kernel, count), out_shape=(jax.Sha...  2.05 us

profile of v4, /device:TPU:8, one launch (start us, length us, event | category | flops | bytes accessed | tf_op | source)
XLA Modules:
  0.0 100.4 jit_solution(9034076158002239927)
XLA Ops:
  0.6 97.7 %shard_map.59 = (bf16[8192,256]{1,0:T(8,128)(2,1)S(1)}, bf16[1,1536]{1,0:T(2,128)(2,1)S(1)}) custom-call(bf16[2048,2048]{1,0:T(8,128)(2,1)} %bitcast.3, bf16[2048,1024]{1,0:T(8,128)(2,1)} %w_hbm.1, bf16[1,1536]{1,0:T(2,128)(2,1)} %q_ref.1, f32[1,24]{1,0:T(1,128)} %bitcast.4), custom_call_target="tpu_custom_call" | custom-call | tf_op jit(solution)/shard_map/pallas_call | solution.py:377
  98.3 2.1 %shard_map.60 = (bf16[8192,256]{1,0:T(8,128)(2,1)}, bf16[1,1536]{1,0:T(2,128)(2,1)}) custom-call(bf16[8192,256]{1,0:T(8,128)(2,1)S(1)} %get-tuple-element.6.got, bf16[1,1536]{1,0:T(2,128)(2,1)S(1)} %get-tuple-element.7.read), custom_call_target="tpu_custom_call" | custom-call | tf_op jit(solution)/shard_map/pallas_call | solution.py:408

commit v5 on v4

--- a/solution.py
+++ b/solution.py
@@ -346,8 +346,8 @@
         at = pl.ds(k * rows, rows)
         copies.append(pltpu.make_async_copy(got.at[at, :], cache.at[at, :], sems.at[k]))
     copies.append(pltpu.make_async_copy(read, read_out, sems.at[count]))
-    for copy in copies:
-        copy.start()
+    for k, copy in enumerate(copies):
+        copy.start(priority=k % 2)
     for copy in copies:
         copy.wait()
 

time: 101 us -> 101 us (level)
  no operation moved by 1% of the time
where the time goes in v5:
time: 101 us; the launch traced here: 100 us
  Pallas kernels  99.7 us (99%)
    pallas_call x1, Pallas kernels, local(): pl.pallas_call(functools.partial(exchange_kernel, count), out_shape=(pltp...  97.7 us
    pallas_call x1, Pallas kernels, local(): pl.pallas_call(functools.partial(place_kernel, count), out_shape=(jax.Sha...  2.06 us

profile of v5, /device:TPU:8, one launch (start us, length us, event | category | flops | bytes accessed | tf_op | source)
XLA Modules:
  0.0 100.4 jit_solution(17478984475764979508)
XLA Ops:
  0.6 97.7 %shard_map.59 = (bf16[8192,256]{1,0:T(8,128)(2,1)S(1)}, bf16[1,1536]{1,0:T(2,128)(2,1)S(1)}) custom-call(bf16[2048,2048]{1,0:T(8,128)(2,1)} %bitcast.3, bf16[2048,1024]{1,0:T(8,128)(2,1)} %w_hbm.1, bf16[1,1536]{1,0:T(2,128)(2,1)} %q_ref.1, f32[1,24]{1,0:T(1,128)} %bitcast.4), custom_call_target="tpu_custom_call" | custom-call | tf_op jit(solution)/shard_map/pallas_call | solution.py:377
  98.3 2.1 %shard_map.60 = (bf16[8192,256]{1,0:T(8,128)(2,1)}, bf16[1,1536]{1,0:T(2,128)(2,1)}) custom-call(bf16[8192,256]{1,0:T(8,128)(2,1)S(1)} %get-tuple-element.6.got, bf16[1,1536]{1,0:T(2,128)(2,1)S(1)} %get-tuple-element.7.read), custom_call_target="tpu_custom_call" | custom-call | tf_op jit(solution)/shard_map/pallas_call | solution.py:408
